TPU v7x, 32 devices: a whole 2x2x4 slice. The times are simulated.
32 devices in a mesh: ra: 4 (over y, x), cb: 8 (over z, core).
Axes of the slice: x: 2, y: 2, z: 4, core: 2. Of those that a mesh axis runs over, the one named last changes fastest.
Arguments:
- tokens: bfloat16 [512, 4096], P(None, 'ra'), may hold values from -40 to 40, as said below
- norm_gain: float32 [2, 4096], P(None, 'ra'), may hold values from 0.1 to 1.9
- gate_weight: bfloat16 [2, 4096, 11264], P(None, 'ra', 'cb'), may hold values from -0.09375 to 0.09375
- up_weight: bfloat16 [2, 4096, 11264], P(None, 'ra', 'cb'), may hold values from -0.09375 to 0.09375
- down_weight: bfloat16 [2, 11264, 4096], P(None, 'cb', 'ra'), may hold values from -0.0546875 to 0.0546875
Outputs:
- result: bfloat16 [512, 4096], P(None, 'ra')
Inputs may be any that keep to these rules, and one draw needn't show every extreme that they name: `tokens`: features come in blocks of 32 with scales that differ from block to block by up to a factor of 16.
All inputs are finite; a program needn't handle non-finite values.
Results may differ from a plain program's by a relative error of at most 0.0075.
Values may be sent and summed in bfloat16 or wider, within the bound.
A program may use at most 64 MiB of HBM per device.

v0:
```python
import jax
import jax.numpy as jnp
from jax import lax
from jax.sharding import PartitionSpec as P

D = 4096
LAYERS = 2
epsilon = 1e-06
keep_share = 0.5


def body(tokens, norm_gain, gate_weight, up_weight, down_weight):
    stream = tokens
    for layer in range(LAYERS):
        widened = stream.astype(jnp.float32)
        squares = jnp.sum(widened * widened, axis=1)
        normed = (widened * norm_gain[layer]).astype(jnp.bfloat16)
        gate_part = jnp.dot(normed, gate_weight[layer], preferred_element_type=jnp.float32)
        up_part = jnp.dot(normed, up_weight[layer], preferred_element_type=jnp.float32)
        total = lax.psum(squares, "ra")
        gate_share, up_share = (
            lax.psum_scatter(gate_part, "ra", scatter_dimension=1, tiled=True),
            lax.psum_scatter(up_part, "ra", scatter_dimension=1, tiled=True),
        )
        scale = lax.rsqrt(total / D + epsilon)[:, None]
        share = (jax.nn.silu(gate_share * scale) * (up_share * scale)).astype(jnp.bfloat16)
        hidden = lax.all_gather(share, "ra", axis=1, tiled=True)
        partial_down = jnp.dot(hidden, down_weight[layer], preferred_element_type=jnp.float32)
        branch = lax.psum(partial_down, "cb")
        stream = (keep_share * widened + branch).astype(jnp.bfloat16)
    return stream


def solution(mesh):
    placed = (
        P(None, "ra"),
        P(None, "ra"),
        P(None, "ra", "cb"),
        P(None, "ra", "cb"),
        P(None, "cb", "ra"),
    )
    return jax.shard_map(body, mesh=mesh, in_specs=placed, out_specs=P(None, "ra"), check_vma=False)
```

profile of v0, /device:TPU:0, one launch (start us, length us, event | category | flops | bytes accessed | tf_op | source)
XLA Modules:
  0.0 411.4 jit_solution(7383496427016766130)
XLA Ops:
  6.5 0.8 fusion.31
  7.3 5.4 %fusion.8 = f32[512,1408]{0,1:T(8,128)} fusion(bf16[2,1024,1408]{2,1,0:T(8,128)(2,1)} %param.8, bf16[512,1024]{1,0:T(8,128)(2,1)} %param.5, f32[1024]{0:T(1024)S(1)} %bitcast.24), kind=kOutput, calls=%fused_computation.14 | convolution fusion | flops 1477967872 | bytes 6819840 | tf_op jit(solution)/shard_map/dot_general | solution.py:19
  12.7 0.0 reduce-scatter.7.cloned.1.call-update
  12.8 0.0 reduce-scatter.5.cloned.1.call-start
  12.8 1.1 copy-done
  14.0 5.1 %fusion.10 = f32[512,1408]{0,1:T(8,128)} fusion(bf16[2,1024,1408]{2,1,0:T(8,128)(2,1)} %param.7, bf16[512,1024]{1,0:T(8,128)(2,1)S(1)} %copy-done, f32[1024]{0:T(1024)S(1)} %bitcast.25), kind=kOutput, calls=%fused_computation.16 | convolution fusion | flops 1477967872 | bytes 6819840 | tf_op jit(solution)/shard_map/dot_general | solution.py:18
  19.1 0.0 reduce-scatter.5.cloned.1.call-update
  19.1 0.0 all-gather.3.cloned.1.call-start
  19.2 0.3 fusion.21
  19.5 11.9 %psum.28 = f32[512]{0:T(512)S(1)} all-reduce(f32[512]{0:T(512)S(1)} %fusion.21), channel_id=1, replica_groups=mesh['ra'=4,'cb'=8] {'ra'}, use_global_device_ids=true, to_apply=%region_2.0 | all-reduce | flops 512 | bytes 4096 | tf_op jit(solution)/shard_map/psum | solution.py:20
  31.4 26.3 %reduce-scatter.7.cloned.1.call-done = f32[512,352]{0,1:T(8,128)} async-done(((f32[512,1408]{0,1:T(8,128)}), f32[512,352]{0,1:T(8,128)}) %reduce-scatter.7.cloned.1.call-update) | async-done | bytes 720912 | tf_op jit(solution)/shard_map/reduce_scatter | solution.py:23
  57.6 44.8 %reduce-scatter.5.cloned.1.call-done = f32[512,352]{0,1:T(8,128)} async-done(((f32[512,1408]{0,1:T(8,128)}), f32[512,352]{0,1:T(8,128)}) %reduce-scatter.5.cloned.1.call-update) | async-done | bytes 720912 | tf_op jit(solution)/shard_map/reduce_scatter | solution.py:22
  102.4 2.3 multiply_convert_fusion.1
  104.7 0.0 all-reduce.3.cloned.1.call-start
  104.8 29.8 %all-gather.3.cloned.1.call-done = bf16[512,1408]{0,1:T(8,128)(2,1)} async-done(((bf16[512,352]{0,1:T(8,128)(2,1)}), bf16[512,1408]{0,1:T(8,128)(2,1)}) %all-gather.3.cloned.1.call-update) | async-done | bytes 1441808 | tf_op jit(solution)/shard_map/all_gather | solution.py:27
  134.6 5.4 %fusion.6 = f32[512,1024]{1,0:T(8,128)} fusion(bf16[512,1408]{0,1:T(8,128)(2,1)} %all-gather.3.cloned.1.call-done, bf16[2,1408,1024]{2,1,0:T(8,128)(2,1)} %param.9), kind=kOutput, calls=%fused_computation.12 | convolution fusion | flops 1476395008 | bytes 6422528 | tf_op jit(solution)/shard_map/dot_general | solution.py:28
  140.1 0.0 reduce-scatter.9.cloned.1.call-start
  140.1 65.2 %all-reduce.3.cloned.1.call-done = f32[512,1024]{1,0:T(8,128)} async-done(((f32[512,1024]{1,0:T(8,128)}), f32[512,1024]{1,0:T(8,128)}) %all-reduce.3.cloned.1.call-update) | async-done | bytes 2097168 | tf_op jit(solution)/shard_map/psum | solution.py:29
  205.3 2.0 fusion.25
  207.4 5.1 %fusion.4 = f32[512,1408]{0,1:T(8,128)} fusion(bf16[2,1024,1408]{2,1,0:T(8,128)(2,1)} %param.7, bf16[512,1024]{1,0:T(8,128)(2,1)S(1)} %get-tuple-element.6, f32[1024]{0:T(1024)S(1)} %bitcast.22), kind=kOutput, calls=%fused_computation.10 | convolution fusion | flops 1477967872 | bytes 6819840 | tf_op jit(solution)/shard_map/dot_general | solution.py:18
  212.5 0.0 reduce-scatter.11.cloned.1.call-start
  212.5 5.1 %fusion.2 = f32[512,1408]{0,1:T(8,128)} fusion(bf16[2,1024,1408]{2,1,0:T(8,128)(2,1)} %param.8, bf16[512,1024]{1,0:T(8,128)(2,1)S(1)} %get-tuple-element.6, f32[1024]{0:T(1024)S(1)} %bitcast.23), kind=kOutput, calls=%fused_computation.8 | convolution fusion | flops 1477967872 | bytes 6819840 | tf_op jit(solution)/shard_map/dot_general | solution.py:19
  217.7 0.0 all-gather.5.cloned.1.call-start
  217.7 10.4 %psum.30 = f32[512]{0:T(512)S(1)} all-reduce(f32[512]{0:T(512)S(1)} %get-tuple-element.5), channel_id=1, replica_groups=mesh['ra'=4,'cb'=8] {'ra'}, use_global_device_ids=true, to_apply=%region_7.8 | all-reduce | flops 512 | bytes 4096 | tf_op jit(solution)/shard_map/psum | solution.py:20
  228.1 26.0 %reduce-scatter.9.cloned.1.call-done = f32[512,352]{0,1:T(8,128)} async-done(((f32[512,1408]{0,1:T(8,128)}), f32[512,352]{0,1:T(8,128)}) %reduce-scatter.9.cloned.1.call-update) | async-done | bytes 720912 | tf_op jit(solution)/shard_map/reduce_scatter | solution.py:22
  254.1 44.7 %reduce-scatter.11.cloned.1.call-done = f32[512,352]{0,1:T(8,128)} async-done(((f32[512,1408]{0,1:T(8,128)}), f32[512,352]{0,1:T(8,128)}) %reduce-scatter.11.cloned.1.call-update) | async-done | bytes 720912 | tf_op jit(solution)/shard_map/reduce_scatter | solution.py:23
  298.8 2.3 multiply_convert_fusion
  301.1 0.0 all-reduce.5.cloned.1.call-start
  301.1 29.9 %all-gather.5.cloned.1.call-done = bf16[512,1408]{0,1:T(8,128)(2,1)} async-done(((bf16[512,352]{0,1:T(8,128)(2,1)}), bf16[512,1408]{0,1:T(8,128)(2,1)}) %all-gather.5.cloned.1.call-update) | async-done | bytes 1441808 | tf_op jit(solution)/shard_map/all_gather | solution.py:27
  331.0 5.4 %fusion = f32[512,1024]{1,0:T(8,128)} fusion(bf16[512,1408]{0,1:T(8,128)(2,1)} %all-gather.5.cloned.1.call-done, bf16[2,1408,1024]{2,1,0:T(8,128)(2,1)} %param.9), kind=kOutput, calls=%fused_computation.6 | convolution fusion | flops 1476395008 | bytes 6422528 | tf_op jit(solution)/shard_map/dot_general | solution.py:28
  336.5 65.2 %all-reduce.5.cloned.1.call-done = f32[512,1024]{1,0:T(8,128)} async-done(((f32[512,1024]{1,0:T(8,128)}), f32[512,1024]{1,0:T(8,128)}) %all-reduce.5.cloned.1.call-update) | async-done | bytes 2097168 | tf_op jit(solution)/shard_map/psum | solution.py:29
  401.7 2.9 fusion.23
  (10 shorter events, 0.1 us)
Async XLA Ops:
  6.5 51.1 %reduce-scatter.7.cloned.1.call-start = ((), (), s32[]{:S(2)}) async-start(), calls=%async_computation.5 | async-start | bytes 3604480 | tf_op jit(solution)/shard_map/reduce_scatter | solution.py:23
  12.7 1.2 copy-start
  12.8 89.7 %reduce-scatter.5.cloned.1.call-start = ((), (), s32[]{:S(2)}) async-start(), calls=%async_computation.4 | async-start | bytes 3604480 | tf_op jit(solution)/shard_map/reduce_scatter | solution.py:22
  19.1 115.5 %all-gather.3.cloned.1.call-start = ((), (), s32[]{:S(2)}) async-start(), calls=%async_computation.6 | async-start | bytes 1802240 | tf_op jit(solution)/shard_map/all_gather | solution.py:27
  104.7 100.6 %all-reduce.3.cloned.1.call-start = ((), (), s32[]{:S(2)}) async-start(), calls=%async_computation.7 | async-start | bytes 4194304 | tf_op jit(solution)/shard_map/psum | solution.py:29
  140.1 114.1 %reduce-scatter.9.cloned.1.call-start = ((), (), s32[]{:S(2)}) async-start(), calls=%async_computation.8 | async-start | bytes 3604480 | tf_op jit(solution)/shard_map/reduce_scatter | solution.py:22
  212.5 86.3 %reduce-scatter.11.cloned.1.call-start = ((), (), s32[]{:S(2)}) async-start(), calls=%async_computation.9 | async-start | bytes 3604480 | tf_op jit(solution)/shard_map/reduce_scatter | solution.py:23
  217.7 113.3 %all-gather.5.cloned.1.call-start = ((), (), s32[]{:S(2)}) async-start(), calls=%async_computation.10 | async-start | bytes 1802240 | tf_op jit(solution)/shard_map/all_gather | solution.py:27
  301.1 100.6 %all-reduce.5.cloned.1.call-start = ((), (), s32[]{:S(2)}) async-start(), calls=%async_computation.11 | async-start | bytes 4194304 | tf_op jit(solution)/shard_map/psum | solution.py:29
Sparse Core Ops, SparseCore 0:
  12.9 44.7 reduce-scatter.6
  60.7 41.7 reduce-scatter.4
  104.9 29.7 all-gather.2
  140.2 65.0 all-reduce.2
  212.6 41.4 reduce-scatter.8
  257.0 41.7 reduce-scatter.10
  301.2 29.7 all-gather.4
  336.6 65.0 all-reduce.4
where the time goes:
time: 412 us; the launch traced here: 411 us
  waiting for transfers between devices  332 us (81%)
  matrix products  31.6 us (8%)
  blocking collectives  22.2 us (5%)
  between operations  13.5 us (3%)
  other arithmetic  9.81 us (2%)
    psum x2, waiting for transfers between devices, body(): branch = lax.psum(partial_down, 'cb')  130 us
    reduce_scatter x2, waiting for transfers between devices, body(): lax.psum_scatter(up_part, 'ra', scatter_dimension=1, tiled=True)  70.9 us
    reduce_scatter x2, waiting for transfers between devices, body(): lax.psum_scatter(gate_part, 'ra', scatter_dimension=1, tiled=True)  70.8 us
    all_gather x2, waiting for transfers between devices, body(): hidden = lax.all_gather(share, 'ra', axis=1, tiled=True)  59.7 us
    psum x2, blocking collectives, body(): total = lax.psum(squares, 'ra')  22.2 us
    dot_general x2, matrix products, body(): jnp.dot(hidden, down_weight[layer], preferred_element_type=jnp.float32)  10.8 us
    dot_general x2, matrix products, body(): jnp.dot(normed, up_weight[layer], preferred_element_type=jnp.float32)  10.6 us
    dot_general x2, matrix products, body(): jnp.dot(normed, gate_weight[layer], preferred_element_type=jnp.float32)  10.2 us
  transfers between devices with their start and end apart: 8, of which 8 were waited for; matrix products, arithmetic and copies ran while one was open for 3% of the time, Pallas kernels for 0%

commit v1 on v0

--- a/solution.py
+++ b/solution.py
@@ -1,3 +1,4 @@
+import functools
 import jax
 import jax.numpy as jnp
 from jax import lax
@@ -9,6 +10,14 @@
 keep_share = 0.5
 
 
+def enter_the_columns(in_array, comm_axis):
+    parts_out = lax.all_gather(in_array, comm_axis)
+    return jnp.sum(parts_out, 0)
+
+
+match_signs = functools.partial(enter_the_columns, comm_axis="ra")
+
+
 def body(tokens, norm_gain, gate_weight, up_weight, down_weight):
     stream = tokens
     for layer in range(LAYERS):
@@ -17,7 +26,7 @@
         normed = (widened * norm_gain[layer]).astype(jnp.bfloat16)
         gate_part = jnp.dot(normed, gate_weight[layer], preferred_element_type=jnp.float32)
         up_part = jnp.dot(normed, up_weight[layer], preferred_element_type=jnp.float32)
-        total = lax.psum(squares, "ra")
+        total = match_signs(squares)
         gate_share, up_share = (
             lax.psum_scatter(gate_part, "ra", scatter_dimension=1, tiled=True),
             lax.psum_scatter(up_part, "ra", scatter_dimension=1, tiled=True),

time: 412 us -> 412 us (level)
    psum x2 -> x0, blocking collectives: 22.2 us -> none  [body(): total = lax.psum(squares, 'ra')]
    all_gather x0 -> x2, blocking collectives: none -> 18.2 us  [enter_the_columns(): parts_out = lax.all_gather(in_array, comm_axis)]
where the time goes in v1:
time: 412 us; the launch traced here: 411 us
  waiting for transfers between devices  336 us (82%)
  matrix products  31.6 us (8%)
  blocking collectives  18.2 us (4%)
  between operations  13.5 us (3%)
  other arithmetic  9.85 us (2%)
    psum x2, waiting for transfers between devices, body(): branch = lax.psum(partial_down, 'cb')  130 us
    reduce_scatter x2, waiting for transfers between devices, body(): lax.psum_scatter(up_part, 'ra', scatter_dimension=1, tiled=True)  72.7 us
    reduce_scatter x2, waiting for transfers between devices, body(): lax.psum_scatter(gate_part, 'ra', scatter_dimension=1, tiled=True)  72.7 us
    all_gather x2, waiting for transfers between devices, body(): hidden = lax.all_gather(share, 'ra', axis=1, tiled=True)  59.7 us
    all_gather x2, blocking collectives, enter_the_columns(): parts_out = lax.all_gather(in_array, comm_axis)  18.2 us
    dot_general x2, matrix products, body(): jnp.dot(hidden, down_weight[layer], preferred_element_type=jnp.float32)  10.8 us
    dot_general x2, matrix products, body(): jnp.dot(normed, up_weight[layer], preferred_element_type=jnp.float32)  10.6 us
    dot_general x2, matrix products, body(): jnp.dot(normed, gate_weight[layer], preferred_element_type=jnp.float32)  10.2 us
  transfers between devices with their start and end apart: 8, of which 8 were waited for; matrix products, arithmetic and copies ran while one was open for 3% of the time, Pallas kernels for 0%

profile of v1, /device:TPU:0, one launch (start us, length us, event | category | flops | bytes accessed | tf_op | source)
XLA Modules:
  0.0 411.0 jit_solution(12829749652026865990)
XLA Ops:
  6.5 0.8 fusion.31
  7.3 5.4 %fusion.8 = f32[512,1408]{0,1:T(8,128)} fusion(bf16[2,1024,1408]{2,1,0:T(8,128)(2,1)} %param.8, bf16[512,1024]{1,0:T(8,128)(2,1)} %param.5, f32[1024]{0:T(1024)S(1)} %bitcast.28), kind=kOutput, calls=%fused_computation.14 | convolution fusion | flops 1477967872 | bytes 6819840 | tf_op jit(solution)/shard_map/dot_general | solution.py:28
  12.7 0.0 reduce-scatter.7.cloned.1.call-update
  12.8 0.0 reduce-scatter.5.cloned.1.call-start
  12.8 1.1 copy-done
  14.0 5.1 %fusion.10 = f32[512,1408]{0,1:T(8,128)} fusion(bf16[2,1024,1408]{2,1,0:T(8,128)(2,1)} %param.7, bf16[512,1024]{1,0:T(8,128)(2,1)S(1)} %copy-done, f32[1024]{0:T(1024)S(1)} %bitcast.29), kind=kOutput, calls=%fused_computation.16 | convolution fusion | flops 1477967872 | bytes 6819840 | tf_op jit(solution)/shard_map/dot_general | solution.py:27
  19.1 0.0 reduce-scatter.5.cloned.1.call-update
  19.1 0.0 all-gather.7.cloned.1.call-start
  19.2 0.3 fusion.21
  19.5 9.9 %all-gather.2 = f32[4,1,512]{2,1,0:T(1,128)S(1)} all-gather(f32[1,1,512]{2,1,0:T(1,128)S(1)} %bitcast.25), channel_id=2, replica_groups=mesh['ra'=4,'cb'=8] {'ra'}, dimensions={0}, use_global_device_ids=true | all-gather | bytes 10240 | tf_op jit(solution)/shard_map/all_gather | solution.py:14
  29.4 28.1 %reduce-scatter.7.cloned.1.call-done = f32[512,352]{0,1:T(8,128)} async-done(((f32[512,1408]{0,1:T(8,128)}), f32[512,352]{0,1:T(8,128)}) %reduce-scatter.7.cloned.1.call-update) | async-done | bytes 720912 | tf_op jit(solution)/shard_map/reduce_scatter | solution.py:32
  57.4 44.8 %reduce-scatter.5.cloned.1.call-done = f32[512,352]{0,1:T(8,128)} async-done(((f32[512,1408]{0,1:T(8,128)}), f32[512,352]{0,1:T(8,128)}) %reduce-scatter.5.cloned.1.call-update) | async-done | bytes 720912 | tf_op jit(solution)/shard_map/reduce_scatter | solution.py:31
  102.3 2.3 multiply_convert_fusion.1
  104.6 0.0 all-reduce.3.cloned.1.call-start
  104.6 29.8 %all-gather.7.cloned.1.call-done = bf16[512,1408]{0,1:T(8,128)(2,1)} async-done(((bf16[512,352]{0,1:T(8,128)(2,1)}), bf16[512,1408]{0,1:T(8,128)(2,1)}) %all-gather.7.cloned.1.call-update) | async-done | bytes 1441808 | tf_op jit(solution)/shard_map/all_gather | solution.py:36
  134.4 5.4 %fusion.6 = f32[512,1024]{1,0:T(8,128)} fusion(bf16[512,1408]{0,1:T(8,128)(2,1)} %all-gather.7.cloned.1.call-done, bf16[2,1408,1024]{2,1,0:T(8,128)(2,1)} %param.9), kind=kOutput, calls=%fused_computation.12 | convolution fusion | flops 1476395008 | bytes 6422528 | tf_op jit(solution)/shard_map/dot_general | solution.py:37
  139.9 0.0 reduce-scatter.9.cloned.1.call-start
  139.9 65.2 %all-reduce.3.cloned.1.call-done = f32[512,1024]{1,0:T(8,128)} async-done(((f32[512,1024]{1,0:T(8,128)}), f32[512,1024]{1,0:T(8,128)}) %all-reduce.3.cloned.1.call-update) | async-done | bytes 2097168 | tf_op jit(solution)/shard_map/psum | solution.py:38
  205.1 2.0 fusion.25
  207.1 5.1 %fusion.4 = f32[512,1408]{0,1:T(8,128)} fusion(bf16[2,1024,1408]{2,1,0:T(8,128)(2,1)} %param.7, bf16[512,1024]{1,0:T(8,128)(2,1)S(1)} %get-tuple-element.6, f32[1024]{0:T(1024)S(1)} %bitcast.26), kind=kOutput, calls=%fused_computation.10 | convolution fusion | flops 1477967872 | bytes 6819840 | tf_op jit(solution)/shard_map/dot_general | solution.py:27
  212.2 0.0 reduce-scatter.11.cloned.1.call-start
  212.3 5.1 %fusion.2 = f32[512,1408]{0,1:T(8,128)} fusion(bf16[2,1024,1408]{2,1,0:T(8,128)(2,1)} %param.8, bf16[512,1024]{1,0:T(8,128)(2,1)S(1)} %get-tuple-element.6, f32[1024]{0:T(1024)S(1)} %bitcast.27), kind=kOutput, calls=%fused_computation.8 | convolution fusion | flops 1477967872 | bytes 6819840 | tf_op jit(solution)/shard_map/dot_general | solution.py:28
  217.5 0.0 all-gather.9.cloned.1.call-start
  217.5 8.4 %all-gather.3 = f32[4,1,512]{2,1,0:T(1,128)S(1)} all-gather(f32[1,1,512]{2,1,0:T(1,128)S(1)} %bitcast.24), channel_id=3, replica_groups=mesh['ra'=4,'cb'=8] {'ra'}, dimensions={0}, use_global_device_ids=true | all-gather | bytes 10240 | tf_op jit(solution)/shard_map/all_gather | solution.py:14
  225.9 27.9 %reduce-scatter.9.cloned.1.call-done = f32[512,352]{0,1:T(8,128)} async-done(((f32[512,1408]{0,1:T(8,128)}), f32[512,352]{0,1:T(8,128)}) %reduce-scatter.9.cloned.1.call-update) | async-done | bytes 720912 | tf_op jit(solution)/shard_map/reduce_scatter | solution.py:31
  253.8 44.7 %reduce-scatter.11.cloned.1.call-done = f32[512,352]{0,1:T(8,128)} async-done(((f32[512,1408]{0,1:T(8,128)}), f32[512,352]{0,1:T(8,128)}) %reduce-scatter.11.cloned.1.call-update) | async-done | bytes 720912 | tf_op jit(solution)/shard_map/reduce_scatter | solution.py:32
  298.4 2.3 multiply_convert_fusion
  300.7 0.0 all-reduce.5.cloned.1.call-start
  300.8 29.9 %all-gather.9.cloned.1.call-done = bf16[512,1408]{0,1:T(8,128)(2,1)} async-done(((bf16[512,352]{0,1:T(8,128)(2,1)}), bf16[512,1408]{0,1:T(8,128)(2,1)}) %all-gather.9.cloned.1.call-update) | async-done | bytes 1441808 | tf_op jit(solution)/shard_map/all_gather | solution.py:36
  330.6 5.4 %fusion = f32[512,1024]{1,0:T(8,128)} fusion(bf16[512,1408]{0,1:T(8,128)(2,1)} %all-gather.9.cloned.1.call-done, bf16[2,1408,1024]{2,1,0:T(8,128)(2,1)} %param.9), kind=kOutput, calls=%fused_computation.6 | convolution fusion | flops 1476395008 | bytes 6422528 | tf_op jit(solution)/shard_map/dot_general | solution.py:37
  336.1 65.2 %all-reduce.5.cloned.1.call-done = f32[512,1024]{1,0:T(8,128)} async-done(((f32[512,1024]{1,0:T(8,128)}), f32[512,1024]{1,0:T(8,128)}) %all-reduce.5.cloned.1.call-update) | async-done | bytes 2097168 | tf_op jit(solution)/shard_map/psum | solution.py:38
  401.3 2.9 fusion.23
  (12 shorter events, 0.2 us)
Async XLA Ops:
  6.5 50.9 %reduce-scatter.7.cloned.1.call-start = ((), (), s32[]{:S(2)}) async-start(), calls=%async_computation.5 | async-start | bytes 3604480 | tf_op jit(solution)/shard_map/reduce_scatter | solution.py:32
  12.7 1.2 copy-start
  12.8 89.5 %reduce-scatter.5.cloned.1.call-start = ((), (), s32[]{:S(2)}) async-start(), calls=%async_computation.4 | async-start | bytes 3604480 | tf_op jit(solution)/shard_map/reduce_scatter | solution.py:31
  19.1 115.3 %all-gather.7.cloned.1.call-start = ((), (), s32[]{:S(2)}) async-start(), calls=%async_computation.6 | async-start | bytes 1802240 | tf_op jit(solution)/shard_map/all_gather | solution.py:36
  104.6 100.5 %all-reduce.3.cloned.1.call-start = ((), (), s32[]{:S(2)}) async-start(), calls=%async_computation.7 | async-start | bytes 4194304 | tf_op jit(solution)/shard_map/psum | solution.py:38
  139.9 113.9 %reduce-scatter.9.cloned.1.call-start = ((), (), s32[]{:S(2)}) async-start(), calls=%async_computation.8 | async-start | bytes 3604480 | tf_op jit(solution)/shard_map/reduce_scatter | solution.py:31
  212.2 86.2 %reduce-scatter.11.cloned.1.call-start = ((), (), s32[]{:S(2)}) async-start(), calls=%async_computation.9 | async-start | bytes 3604480 | tf_op jit(solution)/shard_map/reduce_scatter | solution.py:32
  217.5 113.2 %all-gather.9.cloned.1.call-start = ((), (), s32[]{:S(2)}) async-start(), calls=%async_computation.10 | async-start | bytes 1802240 | tf_op jit(solution)/shard_map/all_gather | solution.py:36
  300.7 100.6 %all-reduce.5.cloned.1.call-start = ((), (), s32[]{:S(2)}) async-start(), calls=%async_computation.11 | async-start | bytes 4194304 | tf_op jit(solution)/shard_map/psum | solution.py:38
Sparse Core Ops, SparseCore 0:
  12.9 44.5 reduce-scatter.6
  60.5 41.7 reduce-scatter.4
  104.7 29.7 all-gather.6
  140.0 65.0 all-reduce.2
  212.4 41.3 reduce-scatter.8
  256.7 41.7 reduce-scatter.10
  300.8 29.7 all-gather.8
  336.2 65.0 all-reduce.4
